TPU v7x, 32 devices: a whole 2x2x4 slice. The times are simulated.
32 devices in a mesh: grp: 2 (over y), sp: 4 (over z), tp: 4 (over x, core).
Axes of the slice: x: 2, y: 2, z: 4, core: 2. Of those that a mesh axis runs over, the one named last changes fastest.
Arguments:
- stream: bfloat16 [12288, 4096], P(('grp', 'sp', 'tp')), parts along dimension 0, may hold values from -6 to 6
- norm_gain: float32 [2, 4096], replicated, may hold values from 0.1 to 1.9
- mix_weight: bfloat16 [2, 4, 1024, 1024], P(None, None, 'sp', 'tp'), may hold values from -0.1875 to 0.1875
- branch_scale: float32 [2, 4096], replicated, may hold values from 0.1 to 1.9
Outputs:
- result: bfloat16 [12288, 4096], P(('grp', 'sp', 'tp')), parts along dimension 0
There are 2 independent parts, one for each index of `grp`. A program takes and returns all parts, laid end to end along the dimension named above; an argument that names none is the same for every part. Nothing has to cross between parts.
All inputs are finite; a program needn't handle non-finite values.
Results may differ from a plain program's by a relative error of at most 0.0056.
Values may be sent and summed in bfloat16 or wider, within the bound.
A program may use at most 128 MiB of HBM per device.

v0:
```python
import jax
import jax.numpy as jnp
from jax import lax
from jax.sharding import PartitionSpec as P

GW = 1024
G = 4
LAYERS = 2


epsilon = 1e-06
window_lengths = (2, 4, 8, 16)
halo_rows = 15


def from_behind(block, axis, distance):
    devices = range(lax.axis_size(axis))
    route = [(i - distance, i) for i in devices if i - distance in devices]
    return lax.ppermute(block, axis, route)


def per_device(stream, norm_gain, mix_weight, branch_scale):
    row_count = stream.shape[0]
    feature_width = stream.shape[1]
    offset = lax.axis_index(("sp", "tp")) * row_count
    counts_base = (offset + lax.iota(jnp.int32, row_count)).astype(jnp.float32) + 1.0
    residual = stream.astype(jnp.float32)
    for layer_idx in range(LAYERS):
        scale_rows = lax.rsqrt(jnp.mean(residual * residual, axis=1, keepdims=True) + epsilon)
        normed = (residual * scale_rows * norm_gain[layer_idx]).astype(jnp.bfloat16)
        earlier = from_behind(normed[row_count - halo_rows :], ("sp", "tp"), 1)
        extended = jnp.concatenate([earlier, normed], axis=0).astype(jnp.float32)
        pieces = []
        for group_idx in range(G):
            window_len = window_lengths[group_idx]
            segment = extended[:, group_idx * GW : (group_idx + 1) * GW]
            own_rows = segment[halo_rows:]
            running = own_rows
            for back_step in range(1, window_len):
                running = (
                    running + segment[halo_rows - back_step : halo_rows - back_step + row_count]
                )
            window_mean = running / jnp.minimum(counts_base, float(window_len))[:, None]
            pieces.append((window_mean - own_rows).astype(jnp.bfloat16))
        pooled = jnp.stack(pieces, axis=1)
        weight_shard = mix_weight[layer_idx]
        full_rows = lax.all_gather(weight_shard, "sp", axis=1, tiled=True)
        mixed_out = jnp.einsum(
            "rgc,gcn->rgn",
            pooled,
            lax.all_gather(full_rows, "tp", axis=2, tiled=True),
            preferred_element_type=jnp.float32,
        )
        residual = residual + mixed_out.reshape(row_count, feature_width) * branch_scale[layer_idx]
    return residual.astype(jnp.bfloat16)


def solution(mesh):
    return jax.shard_map(
        per_device,
        mesh=mesh,
        in_specs=(P(("grp", "sp", "tp"), None), P(), P(None, None, "sp", "tp"), P()),
        out_specs=P(("grp", "sp", "tp"), None),
        check_vma=False,
    )
```

profile of v0, /device:TPU:5, one launch (start us, length us, event | category | flops | bytes accessed | tf_op | source)
XLA Modules:
  0.0 247.0 jit_solution(16958773101239605890)
XLA Ops:
  6.5 0.0 all-gather.9.cloned.1.call-start
  6.5 2.2 fusion.69
  8.8 0.0 copy-start.1
  8.8 0.0 all-gather.9.cloned.1.call-update
  8.8 0.0 all-gather.13.cloned.1.call-start
  8.9 0.7 all-gather.13.cloned.1.call-update
  9.6 0.0 all-gather.11.cloned.1.call-start
  9.6 46.0 %all-gather.9.cloned.1.call-done = bf16[1,4,1024,256]{3,2,1,0:T(8,128)(2,1)} async-done(((bf16[1,4,256,256]{3,2,1,0:T(8,128)(2,1)}), bf16[1,4,1024,256]{3,2,1,0:T(8,128)(2,1)}) %all-gather.9.cloned.1.call-update) | async-done | bytes 2097168 | tf_op jit(solution)/shard_map/all_gather | solution.py:47
  55.7 0.0 all-gather.11.cloned.1.call-update
  55.7 0.0 all-gather.15.cloned.1.call-start
  55.7 0.0 copy-done.1
  55.7 0.7 fusion.4
  56.4 0.0 copy-start.3
  56.4 45.3 %all-gather.13.cloned.1.call-done = bf16[1,4,1024,256]{3,2,1,0:T(8,128)(2,1)} async-done(((bf16[1,4,256,256]{3,2,1,0:T(8,128)(2,1)}), bf16[1,4,1024,256]{3,2,1,0:T(8,128)(2,1)}) %all-gather.13.cloned.1.call-update) | async-done | bytes 2097168 | tf_op jit(solution)/shard_map/all_gather | solution.py:47
  101.7 0.0 all-gather.15.cloned.1.call-update
  101.7 0.0 copy-done.3
  101.8 0.0 copy-start.4
  101.8 1.0 fusion.6
  102.8 0.0 copy-start.2
  102.8 1.7 copy-done.2
  104.5 3.8 %collective-permute-start = (bf16[15,4096]{1,0:T(8,128)(2,1)S(1)}, bf16[15,4096]{1,0:T(8,128)(2,1)S(1)}, u32[]{:S(2)}, u32[]{:S(2)}) collective-permute-start(bf16[15,4096]{1,0:T(8,128)(2,1)S(1)} %slice.340), channel_id=1, source_target_pairs={{0,1},{1,2},{2,3},{3,4},{4,5},{5,6},{6,7},{7,8},{8,9},{9,10},{10,1... | collective-permute-start | bytes 368648 | tf_op jit(solution)/shard_map/ppermute | solution.py:19
  108.4 0.0 copy-done.4
  108.4 1.8 collective-permute-done
  110.3 3.3 %maximum_convert_fusion = f32[399,4096]{1,0:T(8,128)S(1)} fusion(bf16[384,4096]{1,0:T(8,128)(2,1)} %copy-done.2, bf16[15,4096]{1,0:T(8,128)(2,1)S(1)} %collective-permute-done), kind=kLoop, calls=%fused_computation.13 | loop fusion | flops 6537216 | bytes 9805824 | tf_op jit(solution)/shard_map/convert_element_type | solution.py:32
  113.6 3.3 %fusion.62 = bf16[384,1,1024]{2,0,1:T(8,128)(2,1)} fusion(f32[384]{0:T(512)S(1)} %fusion.63, f32[399,4096]{1,0:T(8,128)S(1)} %maximum_convert_fusion), kind=kLoop, calls=%fused_computation.114 | loop fusion | flops 7077888 | bytes 25953792 | tf_op jit(solution)/shard_map/stack | solution.py:45
  116.9 3.6 %fusion.56 = (bf16[384,1,1024]{2,0,1:T(8,128)(2,1)}, bf16[384,1,1024]{2,0,1:T(8,128)(2,1)}, bf16[384,1,1024]{2,0,1:T(8,128)(2,1)}) fusion(f32[384]{0:T(512)S(1)} %fusion.66, f32[399,4096]{1,0:T(8,128)S(1)} %maximum_convert_fusion, f32[384]{0:T(512)S(1)} %get-tuple-element.18, f32[384]{0:T(512)S(1)} %get-tuple-element.17), kind=kLoop, calls=%fused_computation.108 | loop fusion | flops 7864320 | bytes 24384000 | tf_op jit(solution)/shard_map/stack | solution.py:45
  120.4 41.7 %all-gather.11.cloned.1.call-done = bf16[1,4,1024,1024]{3,2,1,0:T(8,128)(2,1)} async-done(((bf16[1,4,1024,256]{3,2,1,0:T(8,128)(2,1)}), bf16[1,4,1024,1024]{3,2,1,0:T(8,128)(2,1)}) %all-gather.11.cloned.1.call-update) | async-done | bytes 8388624 | tf_op jit(solution)/shard_map/all_gather | solution.py:51
  162.1 7.8 %fusion.21 = f32[4,48,8,1024]{3,2,1,0:T(8,128)S(1)} fusion(bf16[1,4,1024,1024]{3,2,1,0:T(8,128)(2,1)} %all-gather.11.cloned.1.call-done, bf16[384,1,1024]{2,0,1:T(8,128)(2,1)} %fusion.62, bf16[384,1,1024]{2,0,1:T(8,128)(2,1)} %get-tuple-element.10, bf16[384,1,1024]{2,0,1:T(8,128)(2,1)} %get-tuple-element.9, bf16[384,1,1024]{2,0,1:T(8,128)(2,1)} %get-tuple-element.8), kind=kOutput, calls=%fused_computation.29 | convolution fusion | flops 3225944064 | bytes 17825792 | tf_op jit(solution)/shard_map/rgc,gcn->rgn/dot_general | solution.py:48
  169.8 0.6 copy.7
  170.4 0.0 copy-start
  170.4 1.2 multiply_reduce_fusion
  171.7 2.0 copy-done
  173.7 1.6 multiply_convert_fusion
  175.3 2.3 collective-permute-start.1
  177.6 4.6 %collective-permute-done.1 = bf16[15,4096]{1,0:T(8,128)(2,1)S(1)} collective-permute-done((bf16[15,4096]{1,0:T(8,128)(2,1)S(1)}, bf16[15,4096]{1,0:T(8,128)(2,1)S(1)}, u32[]{:S(2)}, u32[]{:S(2)}) %collective-permute-start.1) | collective-permute-done | bytes 122912 | tf_op jit(solution)/shard_map/ppermute | solution.py:19
  182.3 0.9 maximum_convert_fusion.1
  183.2 3.3 %fusion.61 = bf16[384,1,1024]{2,0,1:T(8,128)(2,1)} fusion(f32[384]{0:T(512)S(1)} %fusion.63, f32[399,4096]{1,0:T(8,128)S(1)} %maximum_convert_fusion.1), kind=kLoop, calls=%fused_computation.113 | loop fusion | flops 7077888 | bytes 25953792 | tf_op jit(solution)/shard_map/stack | solution.py:45
  186.5 3.5 %fusion.55 = (bf16[384,1,1024]{2,0,1:T(8,128)(2,1)}, bf16[384,1,1024]{2,0,1:T(8,128)(2,1)}, bf16[384,1,1024]{2,0,1:T(8,128)(2,1)}) fusion(f32[384]{0:T(512)S(1)} %fusion.66, f32[399,4096]{1,0:T(8,128)S(1)} %maximum_convert_fusion.1, f32[384]{0:T(512)S(1)} %get-tuple-element.18, f32[384]{0:T(512)S(1)} %get-tuple-element.17), kind=kLoop, calls=%fused_computation.107 | loop fusion | flops 7864320 | bytes 24384000 | tf_op jit(solution)/shard_map/stack | solution.py:45
  190.0 32.9 %all-gather.15.cloned.1.call-done = bf16[1,4,1024,1024]{3,2,1,0:T(8,128)(2,1)} async-done(((bf16[1,4,1024,256]{3,2,1,0:T(8,128)(2,1)}), bf16[1,4,1024,1024]{3,2,1,0:T(8,128)(2,1)}) %all-gather.15.cloned.1.call-update) | async-done | bytes 8388624 | tf_op jit(solution)/shard_map/all_gather | solution.py:51
  222.9 0.0 slice-start
  222.9 0.0 slice-start.1
  222.9 7.9 %fusion.26 = f32[4,48,8,1024]{3,2,1,0:T(8,128)S(1)} fusion(bf16[1,4,1024,1024]{3,2,1,0:T(8,128)(2,1)} %all-gather.15.cloned.1.call-done, bf16[384,1,1024]{2,0,1:T(8,128)(2,1)} %fusion.61, bf16[384,1,1024]{2,0,1:T(8,128)(2,1)} %get-tuple-element.7, bf16[384,1,1024]{2,0,1:T(8,128)(2,1)} %get-tuple-element.6, bf16[384,1,1024]{2,0,1:T(8,128)(2,1)} %get-tuple-element.5), kind=kOutput, calls=%fused_computation.30 | convolution fusion | flops 3225944064 | bytes 17825792 | tf_op jit(solution)/shard_map/rgc,gcn->rgn/dot_general | solution.py:48
  230.8 3.4 %copy.8 = f32[4,48,8,1024]{3,2,0,1:T(8,128)} copy(f32[4,48,8,1024]{3,2,1,0:T(8,128)S(1)} %fusion.26) | data formatting | bytes 12582912 | tf_op jit(solution)/shard_map/reshape | solution.py:54
  234.2 0.0 slice-done
  234.2 0.0 slice-done.1
  234.2 6.2 %add_convert_fusion = bf16[384,4096]{1,0:T(8,128)(2,1)} fusion(f32[384,4096]{1,0:T(8,128)} %bitcast.43, f32[4096]{0:T(1024)S(1)} %bitcast.47, f32[384,4096]{1,0:T(8,128)S(1)} %bitcast.42, f32[4096]{0:T(1024)S(1)} %bitcast.46, bf16[384,4096]{1,0:T(8,128)(2,1)S(1)} %copy-done.1), kind=kLoop, calls=%fused_computation.10 | loop fusion | flops 9437184 | bytes 18907136 | tf_op jit(solution)/shard_map/convert_element_type | solution.py:55
  (10 shorter events, 0.2 us)
Async XLA Ops:
  6.5 49.1 %all-gather.9.cloned.1.call-start = ((), (), s32[]{:S(2)}) async-start(), calls=%async_computation | async-start | bytes 2621440 | tf_op jit(solution)/shard_map/all_gather | solution.py:47
  8.8 46.9 %copy-start.1 = (bf16[384,4096]{1,0:T(8,128)(2,1)S(1)}, bf16[384,4096]{1,0:T(8,128)(2,1)}, u32[]{:S(2)}) copy-start(bf16[384,4096]{1,0:T(8,128)(2,1)} %param.4) | copy-start | bytes 9437188
  8.8 92.9 %all-gather.13.cloned.1.call-start = ((), (), s32[]{:S(2)}) async-start(), calls=%async_computation.2 | async-start | bytes 2621440 | tf_op jit(solution)/shard_map/all_gather | solution.py:47
  9.6 152.5 %all-gather.11.cloned.1.call-start = ((), (), s32[]{:S(2)}) async-start(), calls=%async_computation.1 | async-start | bytes 10485760 | tf_op jit(solution)/shard_map/all_gather | solution.py:51
  55.7 167.2 %all-gather.15.cloned.1.call-start = ((), (), s32[]{:S(2)}) async-start(), calls=%async_computation.3 | async-start | bytes 10485760 | tf_op jit(solution)/shard_map/all_gather | solution.py:51
  56.4 45.3 %copy-start.3 = (f32[2,4096]{1,0:T(2,128)S(1)}, f32[2,4096]{1,0:T(2,128)}, u32[]{:S(2)}) copy-start(f32[2,4096]{1,0:T(2,128)} %param.5) | copy-start | bytes 98308
  101.8 6.6 %copy-start.4 = (f32[2,4096]{1,0:T(2,128)S(1)}, f32[2,4096]{1,0:T(2,128)}, u32[]{:S(2)}) copy-start(f32[2,4096]{1,0:T(2,128)} %param.7) | copy-start | bytes 98308
  102.8 1.7 copy-start.2
  104.5 5.8 %collective-permute-start = (bf16[15,4096]{1,0:T(8,128)(2,1)S(1)}, bf16[15,4096]{1,0:T(8,128)(2,1)S(1)}, u32[]{:S(2)}, u32[]{:S(2)}) collective-permute-start(bf16[15,4096]{1,0:T(8,128)(2,1)S(1)} %slice.340), channel_id=1, source_target_pairs={{0,1},{1,2},{2,3},{3,4},{4,5},{5,6},{6,7},{7,8},{8,9},{9,10},{10,1... | collective-permute-start | bytes 368648 | tf_op jit(solution)/shard_map/ppermute | solution.py:19
  170.4 3.3 %copy-start = (f32[4,48,8,1024]{3,2,0,1:T(8,128)}, f32[4,48,8,1024]{3,2,0,1:T(8,128)S(1)}, u32[]{:S(2)}) copy-start(f32[4,48,8,1024]{3,2,0,1:T(8,128)S(1)} %copy.7) | copy-start | bytes 18874372
  175.3 6.9 %collective-permute-start.1 = (bf16[15,4096]{1,0:T(8,128)(2,1)S(1)}, bf16[15,4096]{1,0:T(8,128)(2,1)S(1)}, u32[]{:S(2)}, u32[]{:S(2)}) collective-permute-start(bf16[15,4096]{1,0:T(8,128)(2,1)S(1)} %slice.371), channel_id=1, source_target_pairs={{0,1},{1,2},{2,3},{3,4},{4,5},{5,6},{6,7},{7,8},{8,9},{9,10},{10,1... | collective-permute-start | bytes 368648 | tf_op jit(solution)/shard_map/ppermute | solution.py:19
  222.9 11.3 %slice-start = ((s8[6291456]{0:T(1024)(128)(4,1)}), s8[4194304]{0:T(1024)(128)(4,1)S(1)}, s32[]{:S(2)}) async-start(s8[6291456]{0:T(1024)(128)(4,1)} %bitcast.40), calls=%async_computation.4 | async-start | bytes 8388608
  222.9 11.3 %slice-start.1 = ((s8[6291456]{0:T(1024)(128)(4,1)}), s8[2097152]{0:T(1024)(128)(4,1)S(1)}, s32[]{:S(2)}) async-start(s8[6291456]{0:T(1024)(128)(4,1)} %bitcast.40), calls=%async_computation.5 | async-start | bytes 4194304
Sparse Core Ops, SparseCore 0:
  8.9 46.6 all-gather.8
  57.2 44.4 all-gather.12
  103.3 58.7 all-gather.10
  163.5 59.3 all-gather.14
where the time goes:
time: 249 us; the launch traced here: 247 us
  waiting for transfers between devices  173 us (69%)
  other arithmetic  28.6 us (11%)
  matrix products  15.6 us (6%)
  between operations  13.3 us (5%)
  local copies, waits for them, and re-layouts  10.1 us (4%)
  starting transfers between devices  6.22 us (2%)
    all_gather x2, waiting for transfers between devices, per_device(): full_rows = lax.all_gather(weight_shard, 'sp', axis=1, tiled=True)  91.3 us
    all_gather x2, waiting for transfers between devices, per_device(): lax.all_gather(full_rows, 'tp', axis=2, tiled=True)  74.6 us
    dot_general x2, matrix products, per_device(): jnp.einsum('rgc,gcn->rgn', pooled, lax.all_gather(full_rows, 'tp', axis=2...  15.6 us
    another operation x4, other arithmetic, per_device(): pooled = jnp.stack(pieces, axis=1)  13.6 us
    ppermute x2, waiting for transfers between devices, from_behind(): return lax.ppermute(block, axis, route)  6.48 us
    convert_element_type x1, other arithmetic, per_device(): return residual.astype(jnp.bfloat16)  6.2 us
    ppermute x2, starting transfers between devices, from_behind(): return lax.ppermute(block, axis, route)  6.1 us
  transfers between devices with their start and end apart: 6, of which 6 were waited for; matrix products, arithmetic and copies ran while one was open for 12% of the time, Pallas kernels for 0%

commit v1 on v0

v1 whole, which is shorter than its diff:
```python
import functools

import jax
import jax.numpy as jnp
from jax import lax
from jax.experimental import pallas as pl
from jax.experimental.pallas import tpu as pltpu
from jax.sharding import PartitionSpec as P

MESH = pl.DeviceIdType.MESH
epsilon = 1e-06
window_lengths = (2, 4, 8, 16)
HALO = 16
LANES = 128


def kernel(X, Z, stream, gain, weight, bscale, out, W, S, R, PO, SC, O, recv, send, local, halo_sem):
    LAYERS, G, K, N = weight.shape
    T = 2 * X
    rows, D = stream.shape
    ext = rows + 2 * HALO
    GW = D // G
    y = lax.axis_index("grp")
    z = lax.axis_index("sp")
    t = lax.axis_index("tp")
    x = t // 2
    c = t % 2
    lin = z * T + t
    t_of = lambda xx: xx * 2 + c
    others = [lax.rem(x + k, X) for k in range(1, X)]
    sources = [lax.rem(x + X - k, X) for k in range(1, X)]
    core_dev = {"tp": t + 1 - 2 * c}
    y_dev = {"grp": 1 - y}
    x_devs = [{"tp": t_of(o)} for o in others]
    next_lin = lin + 1
    prev_lin = lin - 1
    next_dev = {"sp": next_lin // T, "tp": lax.rem(next_lin, T)}
    prev_dev = {"sp": (prev_lin + T) // T - 1, "tp": lax.rem(prev_lin + T, T)}
    has_next = lin < Z * T - 1
    has_prev = lin > 0

    own_rows = pltpu.make_async_copy(stream, S.at[pl.ds(2 * HALO, rows)], local.at[0])
    own_rows.start()

    barrier = pltpu.get_barrier_semaphore()

    def greet(dev):
        pl.semaphore_signal(barrier, inc=1, device_id=dev, device_id_type=MESH)

    greet(core_dev)
    greet(y_dev)
    for dev in x_devs:
        greet(dev)
    for dr in (1, -1):
        @pl.when((z + dr >= 0) & (z + dr < Z))
        def _():
            greet({"sp": z + dr})

    @pl.when(has_next)
    def _():
        greet(next_dev)

    @pl.when(has_prev)
    def _():
        greet(prev_dev)

    one = lambda cond: jnp.where(cond, 1, 0)
    pl.semaphore_wait(
        barrier, 2 + (X - 1) + one(z > 0) + one(z < Z - 1) + one(has_next) + one(has_prev)
    )

    def blk(l, g, s, tt):
        return W.at[l, g, tt, pl.ds(pl.multiple_of(s * K, K), K), :]

    def sem_of(l, g, s, tt):
        return recv.at[((l * G + g) * Z + s) * T + tt]

    sites = 2 * (1 + 1 + (X - 1) + 1 + 3 * X + (X - 1) + 1 + X + 2 * (X - 1))

    def copy(l, d, site, g, s, tt, dev, own=False):
        return pltpu.make_async_remote_copy(
            src_ref=weight.at[l, g] if own else blk(l, g, s, tt),
            dst_ref=blk(l, g, s, tt),
            send_sem=send.at[(l * Z + d) * sites + site],
            recv_sem=sem_of(l, g, s, tt),
            device_id=dev,
            device_id_type=MESH,
        )

    def arrived(l, g, s, tt):
        copy(l, 0, 0, g, s, tt, core_dev).wait_recv()

    def do(mode, *args, **kw):
        if mode == "go":
            copy(*args, **kw).start()
        else:
            copy(*args, **kw).wait_send()

    def need(mode, *args):
        if mode == "go":
            arrived(*args)

    def start(mode, l):
        site = 0
        gA, gA2, gB, gB2 = y, 1 - y, 2 + y, 3 - y
        for i, dr in enumerate((1, -1)):
            @pl.when((z + dr >= 0) & (z + dr < Z))
            def _():
                do(mode, l, 0, 2 * i, gB, z, t, {"sp": z + dr}, own=True)
                do(mode, l, 0, 2 * i + 1, gA, z, t, {"sp": z + dr}, own=True)
        site = 4
        for g in (gA, gA2, gB, gB2):
            for dev in x_devs:
                do(mode, l, 0, site, g, z, t, dev, own=True)
                site += 1
        for g in range(G):
            do(mode, l, 0, site, g, z, t, core_dev, own=True)
            site += 1
        return site

    first_sites = 4 + 4 * (X - 1) + 4
    def round0(mode, l, tick):
        site = first_sites
        for s_x in sources:
            st = t_of(s_x)
            need(mode, l, y, z, st)
            for i, dr in enumerate((1, -1)):
                @pl.when((z + dr >= 0) & (z + dr < Z))
                def _():
                    do(mode, l, 0, site + i, y, z, st, {"sp": z + dr})
            do(mode, l, 0, site + 2, y, z, st, core_dev)
            site += 3
        tick()

    def round0_rest(mode, l):
        site = first_sites + 3 * (X - 1)
        for s_x in sources:
            st = t_of(s_x)
            for g in (1 - y, 2 + y, 3 - y):
                need(mode, l, g, z, st)
                do(mode, l, 0, site, g, z, st, core_dev)
                site += 1
        return site

    def z_part(mode, l, d, tick):
        site = 0
        per = 3 + (X - 1)
        for i, dr in enumerate((1, -1)):
            p = z - dr * d
            @pl.when((p >= 0) & (p < Z))
            def _():
                b = i * per
                g = 2 + y
                need(mode, l, g, p, t)
                @pl.when((z + dr >= 0) & (z + dr < Z))
                def _():
                    do(mode, l, d, b, g, p, t, {"sp": z + dr})
                do(mode, l, d, b + 1, g, p, t, y_dev)
                for k, dev in enumerate(x_devs):
                    do(mode, l, d, b + 2 + k, g, p, t, dev)
                do(mode, l, d, b + 2 + X - 1, g, p, t, core_dev)
        site = 2 * per
        tick()
        for j in range(X):
            u = t_of(lax.rem(x + X - j, X))
            for i, dr in enumerate((1, -1)):
                p = z - dr * d
                @pl.when((p >= 0) & (p < Z))
                def _():
                    b = site + i * 3
                    need(mode, l, y, p, u)
                    @pl.when((z + dr >= 0) & (z + dr < Z))
                    def _():
                        do(mode, l, d, b, y, p, u, {"sp": z + dr})
                    do(mode, l, d, b + 1, y, p, u, y_dev)
                    do(mode, l, d, b + 2, y, p, u, core_dev)
            site += 6
            tick()
            if j == 0:
                for i, dr in enumerate((1, -1)):
                    p = z - dr * d
                    @pl.when((p >= 0) & (p < Z))
                    def _():
                        b = site + i * X
                        g = 3 - y
                        need(mode, l, g, p, t)
                        for k, dev in enumerate(x_devs):
                            do(mode, l, d, b + k, g, p, t, dev)
                        do(mode, l, d, b + X - 1, g, p, t, core_dev)
                site += 2 * X
                tick()
        return site

    z_sites = 2 * (3 + (X - 1)) + 6 * X + 2 * X

    def late_part(mode, l, d, tick):
        per = X + 2 * (X - 1)
        for i, dr in enumerate((1, -1)):
            p = z - dr * d
            @pl.when((p >= 0) & (p < Z))
            def _():
                b = z_sites + i * per
                for j in range(X):
                    u = t_of(lax.rem(x + X - j, X))
                    need(mode, l, 1 - y, p, u)
                    do(mode, l, d, b, 1 - y, p, u, core_dev)
                    b += 1
                for g in (2 + y, 3 - y):
                    for s_x in sources:
                        st = t_of(s_x)
                        need(mode, l, g, p, st)
                        do(mode, l, d, b, g, p, st, core_dev)
                        b += 1
            tick()

    nothing = lambda: None

    def scales_first():
        def body(i, _):
            r = pl.ds(pl.multiple_of(i * 16, 16), 16)
            v = S[r, :].astype(jnp.float32)
            m = jnp.sum(v * v, axis=1, keepdims=True) * (1.0 / D)
            SC[r, :] = jnp.broadcast_to(lax.rsqrt(m + epsilon), (16, LANES))
            return 0
        lax.fori_loop(0, ext // 16, body, 0)

    def scales_next():
        m = jnp.sum(SC[HALO:, :], axis=1, keepdims=True) * (1.0 / D)
        SC[HALO:, :] = jnp.broadcast_to(lax.rsqrt(m + epsilon), (ext - HALO, LANES))

    def pool(l, g):
        w = window_lengths[g]
        lo = HALO * l
        n = ext - lo
        position = lin * rows - 2 * HALO + lo + lax.broadcasted_iota(jnp.int32, (n, LANES), 0)
        inv = 1.0 / jnp.clip((position + 1).astype(jnp.float32), 1.0, float(w))

        def body(i, _):
            cols = pl.ds(pl.multiple_of(g * GW + i * LANES, LANES), LANES)
            v = S[lo:, cols].astype(jnp.float32) if l == 0 else R[lo:, cols]
            v = (v * SC[lo:, :] * gain[l : l + 1, cols]).astype(jnp.bfloat16).astype(jnp.float32)
            run = v
            k = 1
            while k < w:
                run = run + pltpu.roll(run, k, 0)
                k *= 2
            PO[lo:, cols] = (run * inv - v).astype(jnp.bfloat16)
            return 0
        lax.fori_loop(0, GW // LANES, body, 0)

    def peer_arrivals(l, g):
        other = 1 - c
        for s in range(Z):
            for xx in range(X):
                arrived(l, g, s, xx * 2 + other)

    def mix(l, g):
        peer_arrivals(l, g)
        lo = HALO * (l + 1)

        def body(i, _):
            cols = pl.ds(pl.multiple_of(g * GW + i * N, N), N)
            acc = jnp.dot(
                PO[lo:, g * GW : (g + 1) * GW], W[l, g, i], preferred_element_type=jnp.float32
            )
            base = S[lo:, cols].astype(jnp.float32) if l == 0 else R[lo:, cols]
            r = base + acc * bscale[l : l + 1, cols]
            if l == LAYERS - 1:
                O[:, cols] = r.astype(jnp.bfloat16)
            else:
                R[lo:, cols] = r
                sq = r * r
                total = SC[lo:, :]
                for q in range(N // LANES):
                    total = total + sq[:, q * LANES : (q + 1) * LANES]
                SC[lo:, :] = total
            return 0
        lax.fori_loop(0, T, body, 0)
        if l == LAYERS - 1:
            put(g).start()

    def put(g):
        part = pl.ds(g * GW, GW)
        return pltpu.make_async_copy(O.at[:, part], out.at[:, part], local.at[2 + g])

    def own_weights():
        return [
            pltpu.make_async_copy(weight.at[l, g], blk(l, g, z, t), sem_of(l, g, z, t))
            for l in range(LAYERS) for g in range(G)
        ]

    def halo():
        return pltpu.make_async_remote_copy(
            src_ref=stream.at[pl.ds(rows - 2 * HALO, 2 * HALO)],
            dst_ref=S.at[pl.ds(0, 2 * HALO)],
            send_sem=halo_sem.at[0],
            recv_sem=halo_sem.at[1],
            device_id=next_dev,
            device_id_type=MESH,
        )

    @pl.when(has_next)
    def _():
        halo().start()

    start("go", 0)
    for o in own_weights():
        o.start()

    @pl.when(jnp.logical_not(has_prev))
    def _():
        S[0 : 2 * HALO, :] = jnp.zeros((2 * HALO, D), S.dtype)

    unrolled = Z <= 4
    own_rows.wait()

    @pl.when(has_prev)
    def _():
        halo().wait_recv()

    pieces = [scales_first] + [functools.partial(pool, 0, g) for g in range(G)]
    tick_on = [True]

    def tick():
        if pieces and tick_on[0]:
            pieces.pop(0)()

    def flush():
        while pieces:
            pieces.pop(0)()

    def clear_sums():
        SC[...] = jnp.zeros_like(SC)

    def rounds(l):
        round0("go", l, tick)
        if unrolled:
            for d in range(1, Z):
                z_part("go", l, d, tick)
                if d == 1:
                    round0_rest("go", l)
                    if l == 0:
                        start("go", 1)
                if d > 1:
                    late_part("go", l, d - 1, tick)
        else:
            round0_rest("go", l)
            if l == 0:
                start("go", 1)
            lax.fori_loop(1, Z, lambda d, _: (z_part("go", l, d, nothing), 0)[1], 0)

    def drain(l):
        if unrolled:
            late_part("go", l, Z - 1, tick)
        else:
            lax.fori_loop(1, Z, lambda d, _: (late_part("go", l, d, nothing), 0)[1], 0)

    tick()
    tick()
    rounds(0)
    flush()
    for o in own_weights():
        o.wait()
    drain(0)
    pieces.append(clear_sums)
    pieces.extend(functools.partial(mix, 0, g) for g in range(G))
    pieces.append(scales_next)
    pieces.extend(functools.partial(pool, 1, g) for g in range(G))
    rounds(1)
    drain(1)
    flush()
    for g in range(G):
        mix(1, g)

    for l in range(LAYERS):
        start("end", l)
        round0("end", l, nothing)
        round0_rest("end", l)

        def ends(d, _):
            z_part("end", l, d, nothing)
            late_part("end", l, d, nothing)
            return 0
        lax.fori_loop(1, Z, ends, 0)

    @pl.when(has_next)
    def _():
        halo().wait_send()

    for g in range(G):
        put(g).wait()


def solution(mesh):
    Z = mesh.shape["sp"]
    X = mesh.shape["tp"] // 2

    def step(stream, norm_gain, mix_weight, branch_scale):
        rows, D = stream.shape
        layers, G, K, N = mix_weight.shape
        T = 2 * X
        ext = rows + 2 * HALO
        any_space = pl.BlockSpec(memory_space=pl.ANY)
        vmem = pl.BlockSpec(memory_space=pltpu.VMEM)
        sites = 2 * (1 + 1 + (X - 1) + 1 + 3 * X + (X - 1) + 1 + X + 2 * (X - 1))
        return pl.pallas_call(
            functools.partial(kernel, X, Z),
            out_shape=jax.ShapeDtypeStruct((rows, D), stream.dtype),
            in_specs=[any_space, vmem, any_space, vmem],
            out_specs=any_space,
            scratch_shapes=[
                pltpu.VMEM((layers, G, T, K * Z, N), mix_weight.dtype),
                pltpu.VMEM((ext, D), stream.dtype),
                pltpu.VMEM((ext, D), jnp.float32),
                pltpu.VMEM((ext, D), jnp.bfloat16),
                pltpu.VMEM((ext, LANES), jnp.float32),
                pltpu.VMEM((rows, D), stream.dtype),
                pltpu.SemaphoreType.DMA((layers * G * Z * T,)),
                pltpu.SemaphoreType.DMA((layers * Z * sites,)),
                pltpu.SemaphoreType.DMA((2 + G,)),
                pltpu.SemaphoreType.DMA((2,)),
            ],
            compiler_params=pltpu.CompilerParams(
                collective_id=0, has_side_effects=True, vmem_limit_bytes=60 * 1024 * 1024
            ),
        )(stream, norm_gain, mix_weight, branch_scale)

    return jax.shard_map(
        step,
        mesh=mesh,
        in_specs=(P(("grp", "sp", "tp"), None), P(), P(None, None, "sp", "tp"), P()),
        out_specs=P(("grp", "sp", "tp"), None),
        check_vma=False,
    )
```

time: 249 us -> 94.7 us (0.38)
  waiting for transfers between devices: 173 us -> 0 us
  Pallas kernels: 0 us -> 90.5 us
  other arithmetic: 28.6 us -> 0 us
  matrix products: 15.6 us -> 0 us
  between operations: 13.3 us -> 0.01 us
  starting transfers between devices: 6.22 us -> 0 us
  local copies, waits for them, and re-layouts: 10.1 us -> 3.91 us
    all_gather x4 -> x0, waiting for transfers between devices: 166 us -> none  [the longest x2 91.3 us: per_device(): full_rows = lax.all_gather(weight_shard, 'sp', axis=1, tiled=True)]
    pallas_call x0 -> x1, Pallas kernels: none -> 90.5 us  [step(): pl.pallas_call(functools.partial(kernel, X, Z), out_shape=jax.ShapeDtypeS...]
    dot_general x2 -> x0, matrix products: 15.6 us -> none  [per_device(): jnp.einsum('rgc,gcn->rgn', pooled, lax.all_gather(full_rows, 'tp', axis=2...]
    another operation x4 -> x0, other arithmetic: 13.6 us -> none  [per_device(): pooled = jnp.stack(pieces, axis=1)]
    convert_element_type x5 -> x0, other arithmetic: 13 us -> none  [the longest x1 6.2 us: per_device(): return residual.astype(jnp.bfloat16)]
    ppermute x2 -> x0, waiting for transfers between devices: 6.48 us -> none  [from_behind(): return lax.ppermute(block, axis, route)]
    ppermute x2 -> x0, starting transfers between devices: 6.1 us -> none  [from_behind(): return lax.ppermute(block, axis, route)]
    reshape x2 -> x0, local copies, waits for them, and re-layouts: 4.01 us -> none  [per_device(): mixed_out.reshape(row_count, feature_width) * branch_scale[layer_idx]]
  transfers between devices with their start and end apart: 6 -> 0, of which waited for: 6 -> 0; matrix products, arithmetic and copies ran while one was open for 12% -> 0% of each run, Pallas kernels for 0% -> 0%
where the time goes in v1:
time: 94.7 us; the launch traced here: 94.5 us
  Pallas kernels  90.5 us (96%)
  local copies, waits for them, and re-layouts  3.91 us (4%)
    pallas_call x1, Pallas kernels, step(): pl.pallas_call(functools.partial(kernel, X, Z), out_shape=jax.ShapeDtypeS...  90.5 us
    unnamed x1, local copies, waits for them, and re-layouts  3.91 us

profile of v1, /device:TPU:5, one launch (start us, length us, event | category | flops | bytes accessed | tf_op | source)
XLA Modules:
  0.0 94.5 jit_solution(3439897902583594521)
XLA Ops:
  0.0 90.5 %shard_map.46 = bf16[384,4096]{1,0:T(8,128)(2,1)} custom-call(bf16[384,4096]{1,0:T(8,128)(2,1)} %stream.1, f32[2,4096]{1,0:T(2,128)} %gain.1, bf16[2,4,256,256]{3,2,1,0:T(8,128)(2,1)} %weight.1, f32[2,4096]{1,0:T(2,128)} %bscale.1), custom_call_target="tpu_custom_call" | custom-call | tf_op jit(solution)/shard_map/pallas_call | solution.py:406
  90.6 3.9 %copy.6 = bf16[384,4096]{1,0:T(8,128)(2,1)} copy(bf16[384,4096]{1,0:T(8,128)(2,1)} %shard_map.46) | data formatting | bytes 6291456

commit v2 on v1

--- a/solution.py
+++ b/solution.py
@@ -14,7 +14,7 @@
 LANES = 128
 
 
-def kernel(X, Z, stream, gain, weight, bscale, out, W, S, R, PO, SC, O, recv, send, local, halo_sem):
+def kernel(X, Z, stream, gain, weight, bscale, O, W, S, R, PO, SC, recv, core_recv, send, local, halo_sem):
     LAYERS, G, K, N = weight.shape
     T = 2 * X
     rows, D = stream.shape
@@ -72,94 +72,78 @@
     def blk(l, g, s, tt):
         return W.at[l, g, tt, pl.ds(pl.multiple_of(s * K, K), K), :]
 
+    SX, SY, SC0, SZ = 0, 2 * (X - 1), 2 * (X - 1) + 1, 2 * (X - 1) + 2
+    per_layer = SZ + 2 * Z
+
     def sem_of(l, g, s, tt):
-        return recv.at[((l * G + g) * Z + s) * T + tt]
-
-    sites = 2 * (1 + 1 + (X - 1) + 1 + 3 * X + (X - 1) + 1 + X + 2 * (X - 1))
-
-    def copy(l, d, site, g, s, tt, dev, own=False):
+        return recv.at[((l * G + g) * Z + s) * X + tt // 2]
+
+    def copy(l, d, link, g, s, tt, dev, own=False):
         return pltpu.make_async_remote_copy(
             src_ref=weight.at[l, g] if own else blk(l, g, s, tt),
             dst_ref=blk(l, g, s, tt),
-            send_sem=send.at[(l * Z + d) * sites + site],
-            recv_sem=sem_of(l, g, s, tt),
+            send_sem=send.at[l * per_layer + link],
+            recv_sem=core_recv.at[l * G + g] if dev is core_dev else sem_of(l, g, s, tt),
             device_id=dev,
             device_id_type=MESH,
         )
 
     def arrived(l, g, s, tt):
-        copy(l, 0, 0, g, s, tt, core_dev).wait_recv()
-
-    def do(mode, *args, **kw):
-        if mode == "go":
-            copy(*args, **kw).start()
-        else:
-            copy(*args, **kw).wait_send()
-
-    def need(mode, *args):
-        if mode == "go":
-            arrived(*args)
-
-    def start(mode, l):
-        site = 0
-        gA, gA2, gB, gB2 = y, 1 - y, 2 + y, 3 - y
+        pltpu.make_async_copy(blk(l, g, s, tt), blk(l, g, s, tt), sem_of(l, g, s, tt)).wait()
+
+    def left(l, link, ref):
+        pltpu.make_async_copy(ref, ref, send.at[l * per_layer + link]).wait()
+
+    def go(*args, **kw):
+        copy(*args, **kw).start()
+
+    def zlink(i, d):
+        return SZ + 2 * d + i
+
+    def start(l):
         for i, dr in enumerate((1, -1)):
             @pl.when((z + dr >= 0) & (z + dr < Z))
             def _():
-                do(mode, l, 0, 2 * i, gB, z, t, {"sp": z + dr}, own=True)
-                do(mode, l, 0, 2 * i + 1, gA, z, t, {"sp": z + dr}, own=True)
-        site = 4
-        for g in (gA, gA2, gB, gB2):
-            for dev in x_devs:
-                do(mode, l, 0, site, g, z, t, dev, own=True)
-                site += 1
+                go(l, 0, zlink(i, 0), 2 + y, z, t, {"sp": z + dr}, own=True)
+                go(l, 0, zlink(i, 0), y, z, t, {"sp": z + dr}, own=True)
+        for g in (y, 1 - y, 2 + y, 3 - y):
+            for k, dev in enumerate(x_devs):
+                go(l, 0, SX + 2 * k, g, z, t, dev, own=True)
         for g in range(G):
-            do(mode, l, 0, site, g, z, t, core_dev, own=True)
-            site += 1
-        return site
-
-    first_sites = 4 + 4 * (X - 1) + 4
-    def round0(mode, l, tick):
-        site = first_sites
+            go(l, 0, SC0, g, z, t, core_dev, own=True)
+
+    def round0(l, tick):
         for s_x in sources:
             st = t_of(s_x)
-            need(mode, l, y, z, st)
+            arrived(l, y, z, st)
             for i, dr in enumerate((1, -1)):
                 @pl.when((z + dr >= 0) & (z + dr < Z))
                 def _():
-                    do(mode, l, 0, site + i, y, z, st, {"sp": z + dr})
-            do(mode, l, 0, site + 2, y, z, st, core_dev)
-            site += 3
+                    go(l, 0, zlink(i, 0), y, z, st, {"sp": z + dr})
+            go(l, 0, SC0, y, z, st, core_dev)
         tick()
 
-    def round0_rest(mode, l):
-        site = first_sites + 3 * (X - 1)
+    def round0_rest(l):
         for s_x in sources:
             st = t_of(s_x)
             for g in (1 - y, 2 + y, 3 - y):
-                need(mode, l, g, z, st)
-                do(mode, l, 0, site, g, z, st, core_dev)
-                site += 1
-        return site
-
-    def z_part(mode, l, d, tick):
-        site = 0
-        per = 3 + (X - 1)
+                arrived(l, g, z, st)
+                go(l, 0, SC0, g, z, st, core_dev)
+
+    def z_part(l, d, tick):
         for i, dr in enumerate((1, -1)):
             p = z - dr * d
             @pl.when((p >= 0) & (p < Z))
             def _():
-                b = i * per
                 g = 2 + y
-                need(mode, l, g, p, t)
+                arrived(l, g, p, t)
                 @pl.when((z + dr >= 0) & (z + dr < Z))
                 def _():
-                    do(mode, l, d, b, g, p, t, {"sp": z + dr})
-                do(mode, l, d, b + 1, g, p, t, y_dev)
+                    go(l, d, zlink(i, d), g, p, t, {"sp": z + dr})
+                go(l, d, SY, g, p, t, y_dev)
                 for k, dev in enumerate(x_devs):
-                    do(mode, l, d, b + 2 + k, g, p, t, dev)
-                do(mode, l, d, b + 2 + X - 1, g, p, t, core_dev)
-        site = 2 * per
+                    go(l, d, SX + 2 * k + 1, g, p, t, dev)
+                go(l, d, SC0, g, p, t, core_dev)
         tick()
         for j in range(X):
             u = t_of(lax.rem(x + X - j, X))
@@ -167,51 +151,53 @@
                 p = z - dr * d
                 @pl.when((p >= 0) & (p < Z))
                 def _():
-                    b = site + i * 3
-                    need(mode, l, y, p, u)
+                    arrived(l, y, p, u)
                     @pl.when((z + dr >= 0) & (z + dr < Z))
                     def _():
-                        do(mode, l, d, b, y, p, u, {"sp": z + dr})
-                    do(mode, l, d, b + 1, y, p, u, y_dev)
-                    do(mode, l, d, b + 2, y, p, u, core_dev)
-            site += 6
+                        go(l, d, zlink(i, d), y, p, u, {"sp": z + dr})
+                    go(l, d, SY, y, p, u, y_dev)
+                    go(l, d, SC0, y, p, u, core_dev)
             tick()
             if j == 0:
                 for i, dr in enumerate((1, -1)):
                     p = z - dr * d
                     @pl.when((p >= 0) & (p < Z))
                     def _():
-                        b = site + i * X
                         g = 3 - y
-                        need(mode, l, g, p, t)
+                        arrived(l, g, p, t)
                         for k, dev in enumerate(x_devs):
-                            do(mode, l, d, b + k, g, p, t, dev)
-                        do(mode, l, d, b + X - 1, g, p, t, core_dev)
-                site += 2 * X
+                            go(l, d, SX + 2 * k + 1, g, p, t, dev)
+                        go(l, d, SC0, g, p, t, core_dev)
                 tick()
-        return site
-
-    z_sites = 2 * (3 + (X - 1)) + 6 * X + 2 * X
-
-    def late_part(mode, l, d, tick):
-        per = X + 2 * (X - 1)
+
+    def late_part(l, d, tick, parts="yx"):
         for i, dr in enumerate((1, -1)):
             p = z - dr * d
             @pl.when((p >= 0) & (p < Z))
             def _():
-                b = z_sites + i * per
-                for j in range(X):
+                for j in range(X) if "y" in parts else ():
                     u = t_of(lax.rem(x + X - j, X))
-                    need(mode, l, 1 - y, p, u)
-                    do(mode, l, d, b, 1 - y, p, u, core_dev)
-                    b += 1
-                for g in (2 + y, 3 - y):
+                    arrived(l, 1 - y, p, u)
+                    go(l, d, SC0, 1 - y, p, u, core_dev)
+                for g in (2 + y, 3 - y) if "x" in parts else ():
                     for s_x in sources:
                         st = t_of(s_x)
-                        need(mode, l, g, p, st)
-                        do(mode, l, d, b, g, p, st, core_dev)
-                        b += 1
+                        arrived(l, g, p, st)
+                        go(l, d, SC0, g, p, st, core_dev)
             tick()
+
+    def sent(l):
+        for k in range(X - 1):
+            left(l, SX + 2 * k, W.at[l, :, 0, pl.ds(0, K)])
+            left(l, SX + 2 * k + 1, W.at[l, pl.ds(0, 2), 0, pl.ds(0, (Z - 1) * K)])
+        left(l, SY, W.at[l, 0, pl.ds(0, X + 1), pl.ds(0, (Z - 1) * K)])
+        left(l, SC0, W.at[l, :, pl.ds(0, X)])
+        for d in range(Z):
+            for i, dr in enumerate((1, -1)):
+                p = z - dr * d
+                @pl.when((p >= 0) & (p < Z) & (z + dr >= 0) & (z + dr < Z))
+                def _():
+                    left(l, zlink(i, d), W.at[l, 0, pl.ds(0, X + 1), pl.ds(0, K)])
 
     nothing = lambda: None
 
@@ -249,10 +235,8 @@
         lax.fori_loop(0, GW // LANES, body, 0)
 
     def peer_arrivals(l, g):
-        other = 1 - c
-        for s in range(Z):
-            for xx in range(X):
-                arrived(l, g, s, xx * 2 + other)
+        ref = W.at[l, g, pl.ds(0, X)]
+        pltpu.make_async_copy(ref, ref, core_recv.at[l * G + g]).wait()
 
     def mix(l, g):
         peer_arrivals(l, g)
@@ -276,12 +260,6 @@
                 SC[lo:, :] = total
             return 0
         lax.fori_loop(0, T, body, 0)
-        if l == LAYERS - 1:
-            put(g).start()
-
-    def put(g):
-        part = pl.ds(g * GW, GW)
-        return pltpu.make_async_copy(O.at[:, part], out.at[:, part], local.at[2 + g])
 
     def own_weights():
         return [
@@ -303,7 +281,7 @@
     def _():
         halo().start()
 
-    start("go", 0)
+    start(0)
     for o in own_weights():
         o.start()
 
@@ -333,27 +311,27 @@
         SC[...] = jnp.zeros_like(SC)
 
     def rounds(l):
-        round0("go", l, tick)
+        round0(l, tick)
         if unrolled:
             for d in range(1, Z):
-                z_part("go", l, d, tick)
+                z_part(l, d, tick)
                 if d == 1:
-                    round0_rest("go", l)
-                    if l == 0:
-                        start("go", 1)
+                    round0_rest(l)
+                if l == 0 and d == 2:
+                    start(1)
                 if d > 1:
-                    late_part("go", l, d - 1, tick)
+                    late_part(l, d - 1, tick)
         else:
-            round0_rest("go", l)
+            round0_rest(l)
             if l == 0:
-                start("go", 1)
-            lax.fori_loop(1, Z, lambda d, _: (z_part("go", l, d, nothing), 0)[1], 0)
+                start(1)
+            lax.fori_loop(1, Z, lambda d, _: (z_part(l, d, nothing), 0)[1], 0)
 
     def drain(l):
         if unrolled:
-            late_part("go", l, Z - 1, tick)
+            late_part(l, Z - 1, tick)
         else:
-            lax.fori_loop(1, Z, lambda d, _: (late_part("go", l, d, nothing), 0)[1], 0)
+            lax.fori_loop(1, Z, lambda d, _: (late_part(l, d, nothing), 0)[1], 0)
 
     tick()
     tick()
@@ -367,28 +345,25 @@
     pieces.append(scales_next)
     pieces.extend(functools.partial(pool, 1, g) for g in range(G))
     rounds(1)
-    drain(1)
     flush()
-    for g in range(G):
-        mix(1, g)
+    if unrolled:
+        late_part(1, Z - 1, nothing, "y")
+        mix(1, 0)
+        mix(1, 1)
+        late_part(1, Z - 1, nothing, "x")
+    else:
+        drain(1)
+        mix(1, 0)
+        mix(1, 1)
+    mix(1, 2)
+    mix(1, 3)
 
     for l in range(LAYERS):
-        start("end", l)
-        round0("end", l, nothing)
-        round0_rest("end", l)
-
-        def ends(d, _):
-            z_part("end", l, d, nothing)
-            late_part("end", l, d, nothing)
-            return 0
-        lax.fori_loop(1, Z, ends, 0)
+        sent(l)
 
     @pl.when(has_next)
     def _():
         halo().wait_send()
-
-    for g in range(G):
-        put(g).wait()
 
 
 def solution(mesh):
@@ -401,23 +376,23 @@
         T = 2 * X
         ext = rows + 2 * HALO
         any_space = pl.BlockSpec(memory_space=pl.ANY)
+        hbm = pl.BlockSpec(memory_space=pltpu.HBM)
         vmem = pl.BlockSpec(memory_space=pltpu.VMEM)
-        sites = 2 * (1 + 1 + (X - 1) + 1 + 3 * X + (X - 1) + 1 + X + 2 * (X - 1))
         return pl.pallas_call(
             functools.partial(kernel, X, Z),
-            out_shape=jax.ShapeDtypeStruct((rows, D), stream.dtype),
-            in_specs=[any_space, vmem, any_space, vmem],
-            out_specs=any_space,
+            out_shape=pltpu.VMEM((rows, D), stream.dtype),
+            in_specs=[hbm, vmem, hbm, vmem],
+            out_specs=vmem,
             scratch_shapes=[
                 pltpu.VMEM((layers, G, T, K * Z, N), mix_weight.dtype),
                 pltpu.VMEM((ext, D), stream.dtype),
                 pltpu.VMEM((ext, D), jnp.float32),
                 pltpu.VMEM((ext, D), jnp.bfloat16),
                 pltpu.VMEM((ext, LANES), jnp.float32),
-                pltpu.VMEM((rows, D), stream.dtype),
-                pltpu.SemaphoreType.DMA((layers * G * Z * T,)),
-                pltpu.SemaphoreType.DMA((layers * Z * sites,)),
-                pltpu.SemaphoreType.DMA((2 + G,)),
+                pltpu.SemaphoreType.DMA((layers * G * Z * X,)),
+                pltpu.SemaphoreType.DMA((layers * G,)),
+                pltpu.SemaphoreType.DMA((layers * (2 * X + 2 * Z),)),
+                pltpu.SemaphoreType.DMA((1,)),
                 pltpu.SemaphoreType.DMA((2,)),
             ],
             compiler_params=pltpu.CompilerParams(

time: 94.7 us -> 85.6 us (0.904); the launches traced: 94.5 us -> 84.4 us
  Pallas kernels: 90.5 us -> 82.7 us
  local copies, waits for them, and re-layouts: 3.91 us -> 1.67 us
    pallas_call x1, Pallas kernels: 90.5 us -> 82.7 us  [step(): pl.pallas_call(functools.partial(kernel, X, Z), out_shape=pltpu.VMEM((row...]
    unnamed x1, local copies, waits for them, and re-layouts: 3.91 us -> 1.67 us
where the time goes in v2:
time: 85.6 us; the launch traced here: 84.4 us
  Pallas kernels  82.7 us (97%)
  local copies, waits for them, and re-layouts  1.67 us (2%)
    pallas_call x1, Pallas kernels, step(): pl.pallas_call(functools.partial(kernel, X, Z), out_shape=pltpu.VMEM((row...  82.7 us

profile of v2, /device:TPU:5, one launch (start us, length us, event | category | flops | bytes accessed | tf_op | source)
XLA Modules:
  0.0 84.4 jit_solution(16735656805126874354)
XLA Ops:
  0.0 82.7 %shard_map.46 = bf16[384,4096]{1,0:T(8,128)(2,1)S(1)} custom-call(bf16[384,4096]{1,0:T(8,128)(2,1)} %stream.1, f32[2,4096]{1,0:T(2,128)} %gain.1, bf16[2,4,256,256]{3,2,1,0:T(8,128)(2,1)} %weight.1, f32[2,4096]{1,0:T(2,128)} %bscale.1), custom_call_target="tpu_custom_call" | custom-call | tf_op jit(solution)/shard_map/pallas_call | solution.py:381
  82.7 1.7 %copy.6 = bf16[384,4096]{1,0:T(8,128)(2,1)} copy(bf16[384,4096]{1,0:T(8,128)(2,1)S(1)} %shard_map.46) | data formatting | bytes 6291456
